TPU v7x, 32 devices: a whole 2x2x4 slice. The times are simulated.
32 devices in a mesh: rep: 2 (over x), fs: 4 (over z), tp: 4 (over y, core).
Axes of the slice: x: 2, y: 2, z: 4, core: 2. Of those that a mesh axis runs over, the one named last changes fastest.
Arguments:
- tokens: bfloat16 [4096, 2048], P(('rep', 'fs', 'tp')), may hold values from -6 to 6
- norm_gain: float32 [2048], replicated, may hold values from 0.1 to 1.9
- gate_weight: float32 [2048, 5632], P('fs', 'tp'), may hold values from -0.125 to 0.125
- gate_scale: float32 [5632], P('tp'), may hold values from 0.5 to 2
- up_weight: float32 [2048, 5632], P('fs', 'tp'), may hold values from -0.125 to 0.125
- up_scale: float32 [5632], P('tp'), may hold values from 0.5 to 2
- down_weight: float32 [5632, 2048], P('tp', 'fs'), may hold values from -0.078125 to 0.078125
- down_scale: float32 [2048], P('fs'), may hold values from 0.5 to 2
Outputs:
- mixed: bfloat16 [4096, 2048], P(('rep', 'fs', 'tp'))
All inputs are finite; a program needn't handle non-finite values.
Results may differ from a plain program's by a relative error of at most 0.014.
Values may be sent and summed in bfloat16 or wider, within the bound.
No kernel may reach another device: no remote copies, remote signals or barrier semaphores. Data moves between devices by JAX's collectives and lax.ppermute only.
A program may use at most 64 MiB of HBM per device.

v0:
```python
import jax
import jax.numpy as jnp
from jax import lax
from jax.sharding import PartitionSpec as P


def shards(
    tokens, norm_gain, gate_weight, gate_scale, up_weight, up_scale, down_weight, down_scale
):
    flat = tokens.astype(jnp.float32)
    mean_square = jnp.mean(flat * flat, axis=-1, keepdims=True)
    inverse = lax.rsqrt(mean_square + 1e-06)
    normed = (flat * inverse * norm_gain).astype(jnp.bfloat16)
    group = lax.all_gather(normed, "tp", axis=0, tiled=True)
    gate_low = gate_weight.astype(jnp.bfloat16)
    up_low = up_weight.astype(jnp.bfloat16)
    down_low = down_weight.astype(jnp.bfloat16)
    gate = jnp.dot(
        group,
        lax.all_gather(gate_low, "fs", axis=0, tiled=True),
        preferred_element_type=jnp.float32,
    )
    up = jnp.dot(
        group, lax.all_gather(up_low, "fs", axis=0, tiled=True), preferred_element_type=jnp.float32
    )
    down_full = lax.all_gather(down_low, "fs", axis=1, tiled=True)
    gate = gate * gate_scale
    up = up * up_scale
    hidden = (jax.nn.silu(gate) * up).astype(jnp.bfloat16)
    scales = lax.all_gather(down_scale, "fs", axis=0, tiled=True)
    total = lax.psum_scatter(
        jnp.dot(hidden, down_full, preferred_element_type=jnp.float32).astype(jnp.bfloat16),
        "tp",
        scatter_dimension=0,
        tiled=True,
    ).astype(jnp.float32)
    return (total * scales).astype(jnp.bfloat16)


def solution(mesh):
    in_specs = (
        P(("rep", "fs", "tp"), None),
        P(),
        P("fs", "tp"),
        P("tp"),
        P("fs", "tp"),
        P("tp"),
        P("tp", "fs"),
        P("fs"),
    )
    out_specs = P(("rep", "fs", "tp"), None)
    return jax.shard_map(shards, mesh=mesh, in_specs=in_specs, out_specs=out_specs, check_vma=False)
```

profile of v0, /device:TPU:0, one launch (start us, length us, event | category | flops | bytes accessed | tf_op | source)
XLA Modules:
  0.0 408.0 jit_solution(18322760977833249545)
XLA Ops:
  6.5 0.0 all-gather.6.cloned.1.call-start
  6.5 1.2 fusion.2
  7.8 2.0 fusion.4
  9.8 0.0 all-gather.6.cloned.1.call-update
  9.8 0.0 copy-start
  9.8 0.0 all-gather.8.cloned.1.call-start
  9.9 3.3 convert_element_type.29
  13.2 0.0 all-gather.8.cloned.1.call-update
  13.2 0.0 all-gather.10.cloned.1.call-start
  13.2 0.0 copy-done
  13.2 1.3 convert_element_type.30
  14.5 0.0 all-gather.10.cloned.1.call-update
  14.5 0.0 copy-start.3
  14.6 0.0 all-gather.12.cloned.1.call-start
  14.6 3.1 convert_element_type.32
  17.8 0.0 all-gather.12.cloned.1.call-update
  17.8 0.0 copy-start.4
  17.8 0.0 reduce-scatter.2.cloned.1.call-start
  17.8 17.4 %all-gather.6.cloned.1.call-done = bf16[512,2048]{1,0:T(8,128)(2,1)} async-done(((bf16[128,2048]{1,0:T(8,128)(2,1)}), bf16[512,2048]{1,0:T(8,128)(2,1)}) %all-gather.6.cloned.1.call-update) | async-done | bytes 2097168 | tf_op jit(solution)/shard_map/all_gather | solution.py:14
  35.3 0.0 copy-start.2
  35.3 108.3 %all-gather.8.cloned.1.call-done = bf16[2048,1408]{1,0:T(8,128)(2,1)} async-done(((bf16[512,1408]{1,0:T(8,128)(2,1)}), bf16[2048,1408]{1,0:T(8,128)(2,1)}) %all-gather.8.cloned.1.call-update) | async-done | bytes 5767184 | tf_op jit(solution)/shard_map/all_gather | solution.py:20
  143.6 0.0 copy-done.3
  143.6 8.2 %convolution_multiply_fusion.1 = f32[512,1408]{1,0:T(8,128)} fusion(bf16[512,2048]{1,0:T(8,128)(2,1)} %all-gather.6.cloned.1.call-done, bf16[2048,1408]{1,0:T(8,128)(2,1)} %all-gather.8.cloned.1.call-done, f32[1408]{0:T(1024)S(1)} %copy-done.3), kind=kOutput, calls=%fused_computation.2 | convolution fusion | flops 2953510912 | bytes 10753536 | tf_op jit(solution)/shard_map/dot_general | solution.py:18
  151.8 0.0 copy-start.1
  151.8 98.3 %all-gather.10.cloned.1.call-done = bf16[2048,1408]{1,0:T(8,128)(2,1)} async-done(((bf16[512,1408]{1,0:T(8,128)(2,1)}), bf16[2048,1408]{1,0:T(8,128)(2,1)}) %all-gather.10.cloned.1.call-update) | async-done | bytes 5767184 | tf_op jit(solution)/shard_map/all_gather | solution.py:24
  250.1 106.4 %all-gather.12.cloned.1.call-done = bf16[1408,2048]{1,0:T(8,128)(2,1)} async-done(((bf16[1408,512]{1,0:T(8,128)(2,1)}), bf16[1408,2048]{1,0:T(8,128)(2,1)}) %all-gather.12.cloned.1.call-update) | async-done | bytes 5767184 | tf_op jit(solution)/shard_map/all_gather | solution.py:26
  356.5 0.0 copy-done.4
  356.5 0.0 copy-done.2
  356.5 13.4 %convolution_convert_fusion = bf16[512,2048]{1,0:T(8,128)(2,1)} fusion(bf16[1408,2048]{1,0:T(8,128)(2,1)} %all-gather.12.cloned.1.call-done, bf16[512,2048]{1,0:T(8,128)(2,1)S(1)} %copy-done.2, bf16[2048,1408]{1,0:T(8,128)(2,1)} %all-gather.10.cloned.1.call-done, f32[512,1408]{1,0:T(8,128)} %convolution_multiply_fusion.1, f32[1408]{0:T(1024)S(1)} %copy-done.4), kind=kOutput, calls=%fused_computation.4 | convolution fusion | flops 5911674880 | bytes 18617856 | tf_op jit(solution)/shard_map/dot_general | solution.py:32
  370.0 0.0 reduce-scatter.2.cloned.1.call-update
  370.0 0.0 copy-done.1
  370.0 11.9 %all-gather = f32[4,1,512]{2,1,0:T(1,128)S(1)} all-gather(f32[1,1,512]{2,1,0:T(1,128)S(1)} %bitcast.8), channel_id=1, replica_groups=mesh['rep'=2,'fs'=4,'tp'=4] {'fs'}, dimensions={0}, use_global_device_ids=true | all-gather | bytes 10240 | tf_op jit(solution)/shard_map/all_gather | solution.py:30
  381.9 17.6 %reduce-scatter.2.cloned.1.call-done = bf16[128,2048]{1,0:T(8,128)(2,1)} async-done(((bf16[512,2048]{1,0:T(8,128)(2,1)}), bf16[128,2048]{1,0:T(8,128)(2,1)}) %reduce-scatter.2.cloned.1.call-update) | async-done | bytes 524304 | tf_op jit(solution)/shard_map/reduce_scatter | solution.py:31
  399.6 1.9 multiply_convert_fusion
  (1 shorter events, 0.0 us)
Async XLA Ops:
  6.5 28.7 %all-gather.6.cloned.1.call-start = ((), (), s32[]{:S(2)}) async-start(), calls=%async_computation.1 | async-start | bytes 2621440 | tf_op jit(solution)/shard_map/all_gather | solution.py:14
  9.8 3.4 copy-start
  9.8 133.7 %all-gather.8.cloned.1.call-start = ((), (), s32[]{:S(2)}) async-start(), calls=%async_computation.2 | async-start | bytes 7208960 | tf_op jit(solution)/shard_map/all_gather | solution.py:20
  13.2 236.9 %all-gather.10.cloned.1.call-start = ((), (), s32[]{:S(2)}) async-start(), calls=%async_computation.3 | async-start | bytes 7208960 | tf_op jit(solution)/shard_map/all_gather | solution.py:24
  14.5 129.0 %copy-start.3 = (f32[1408]{0:T(1024)S(1)}, f32[1408]{0:T(1024)}, u32[]{:S(2)}) copy-start(f32[1408]{0:T(1024)} %param.11) | copy-start | bytes 16900
  14.6 342.0 %all-gather.12.cloned.1.call-start = ((), (), s32[]{:S(2)}) async-start(), calls=%async_computation.4 | async-start | bytes 7208960 | tf_op jit(solution)/shard_map/all_gather | solution.py:26
  17.8 338.7 %copy-start.4 = (f32[1408]{0:T(1024)S(1)}, f32[1408]{0:T(1024)}, u32[]{:S(2)}) copy-start(f32[1408]{0:T(1024)} %param.13) | copy-start | bytes 16900
  17.8 381.8 %reduce-scatter.2.cloned.1.call-start = ((), (), s32[]{:S(2)}) async-start(), calls=%async_computation.5 | async-start | bytes 2621440 | tf_op jit(solution)/shard_map/reduce_scatter | solution.py:31
  35.3 321.2 %copy-start.2 = (bf16[512,2048]{1,0:T(8,128)(2,1)S(1)}, bf16[512,2048]{1,0:T(8,128)(2,1)}, u32[]{:S(2)}) copy-start(bf16[512,2048]{1,0:T(8,128)(2,1)} %all-gather.6.cloned.1.call-done) | copy-start | bytes 6291460
  151.8 218.2 %copy-start.1 = (f32[512]{0:T(512)S(1)}, f32[512]{0:T(512)}, u32[]{:S(2)}) copy-start(f32[512]{0:T(512)} %param.15) | copy-start | bytes 6148
Sparse Core Ops, SparseCore 0:
  9.9 25.2 all-gather.5
  36.8 106.6 all-gather.7
  145.1 104.9 all-gather.9
  251.5 104.9 all-gather.11
  370.1 29.4 reduce-scatter.1
where the time goes:
time: 408 us
  waiting for transfers between devices  348 us (85%)
  matrix products  21.7 us (5%)
  between operations  13.2 us (3%)
  other arithmetic  12.9 us (3%)
  blocking collectives  11.9 us (3%)
    all_gather x1, waiting for transfers between devices, shards(): lax.all_gather(gate_low, 'fs', axis=0, tiled=True)  108 us
    all_gather x1, waiting for transfers between devices, shards(): down_full = lax.all_gather(down_low, 'fs', axis=1, tiled=True)  106 us
    all_gather x1, waiting for transfers between devices, shards(): lax.all_gather(up_low, 'fs', axis=0, tiled=True)  98.3 us
    reduce_scatter x1, waiting for transfers between devices, shards(): lax.psum_scatter(jnp.dot(hidden, down_full, preferred_element_type=jnp.fl...  17.6 us
    all_gather x1, waiting for transfers between devices, shards(): group = lax.all_gather(normed, 'tp', axis=0, tiled=True)  17.4 us
    dot_general x1, matrix products, shards(): jnp.dot(hidden, down_full, preferred_element_type=jnp.float32)  13.4 us
    all_gather x1, blocking collectives, shards(): scales = lax.all_gather(down_scale, 'fs', axis=0, tiled=True)  11.9 us
    dot_general x1, matrix products, shards(): jnp.dot(group, lax.all_gather(gate_low, 'fs', axis=0, tiled=True), prefer...  8.23 us
  transfers between devices with their start and end apart: 5, of which 5 were waited for; matrix products, arithmetic and copies ran while one was open for 4% of the time, Pallas kernels for 0%

commit v1 on v0

v1 whole, which is shorter than its diff:
```python
import functools

import jax
import jax.numpy as jnp
from jax import lax
from jax.experimental import pallas as pl
from jax.experimental.pallas import tpu as pltpu
from jax.sharding import PartitionSpec as P


AXES = ("rep", "fs", "tp")
VMEM_BYTES = 60 * 1024 * 1024
SCALE_ROWS = 16
ROWS_BY_ROWS = (((1,), (1,)), ((), ()))


def hidden_kernel(count, width, aligned, first, last, offsets, *refs):
    refs = list(refs)
    x = refs.pop(0)
    weights = [refs.pop(0) for _ in range(count)]
    sums = None if first else refs.pop(0)
    scales = refs.pop(0) if last else None
    out = refs.pop(0)
    totals = []
    for k in range(2):
        total = None if first else sums[k]
        for i in range(count):
            if aligned:
                part = x[:, pl.ds(pl.multiple_of(offsets[i], width), width)]
            else:
                part = x[:, i * width : (i + 1) * width]
            product = lax.dot_general(
                part, weights[i][k], ROWS_BY_ROWS, preferred_element_type=jnp.float32
            )
            total = product if total is None else total + product
        if not last:
            out[k] = total
        totals.append(total)
    if last:
        gate = totals[0] * scales[0:1, :]
        up = totals[1] * scales[1:2, :]
        out[...] = (gate / (1.0 + jnp.exp(-gate)) * up).astype(out.dtype)


def hidden_part(x, starts, pieces, sums, scales):
    rows, units, width = x.shape[0], pieces[0].shape[1], pieces[0].shape[2]
    first, last = sums is None, scales is not None
    aligned = width % 128 == 0
    if not aligned:
        x = jnp.concatenate([lax.dynamic_slice_in_dim(x, s, width, 1) for s in starts], axis=1)
    block = min(rows, 256)
    once = pl.Buffered(1)
    in_specs = [pl.BlockSpec((block, x.shape[1]), lambda i, o: (i, 0))]
    in_specs += [
        pl.BlockSpec(p.shape, lambda i, o: (0, 0, 0), pipeline_mode=once) for p in pieces
    ]
    operands = [x, *pieces]
    wide = pl.BlockSpec((2, block, units), lambda i, o: (0, i, 0))
    if not first:
        in_specs.append(wide)
        operands.append(sums)
    if last:
        in_specs.append(pl.BlockSpec((2, units), lambda i, o: (0, 0)))
        operands.append(scales)
        out_spec = pl.BlockSpec((block, units), lambda i, o: (i, 0))
        out_shape = jax.ShapeDtypeStruct((rows, units), jnp.bfloat16)
    else:
        out_spec = wide
        out_shape = jax.ShapeDtypeStruct((2, rows, units), jnp.float32)
    return pl.pallas_call(
        functools.partial(hidden_kernel, len(pieces), width, aligned, first, last),
        grid_spec=pltpu.PrefetchScalarGridSpec(
            num_scalar_prefetch=1,
            grid=(rows // block,),
            in_specs=in_specs,
            out_specs=out_spec,
        ),
        out_shape=out_shape,
        compiler_params=pltpu.CompilerParams(vmem_limit_bytes=VMEM_BYTES),
        cost_estimate=pl.CostEstimate(
            flops=4 * rows * width * len(pieces) * units,
            bytes_accessed=4 * width * len(pieces) * units + 8 * rows * units,
            transcendentals=0,
        ),
        name="hidden",
    )(jnp.stack(starts).astype(jnp.int32), *operands)


def plan_of(n):
    mirror, steps = n - 1, []
    for root in (0, mirror):
        held = [root]
        if root:
            steps.append((root, -1, mirror))
        bit = 1
        while bit < n // 2:
            for s in list(held):
                steps.append((s ^ bit, s, bit))
                held.append(s ^ bit)
            bit *= 2
    return steps


def shards(
    sizes,
    tokens,
    norm_gain,
    gate_weight,
    gate_scale,
    up_weight,
    up_scale,
    down_weight,
    down_scale,
):
    reps, n, n_tp = sizes
    half, n_y, mirror = n // 2, n_tp // 2, n - 1
    rep, f = lax.axis_index("rep"), lax.axis_index("fs")
    lower = f < half
    low = jnp.bfloat16
    plan = plan_of(n)
    slots = [0] + [step[0] for step in plan]

    def move(value, target):
        devices = [(r, z, k) for r in range(reps) for z in range(n) for k in range(n_tp)]
        pairs = [(i, devices.index(target(*d))) for i, d in enumerate(devices)]
        return lax.ppermute(value, AXES, pairs)

    def to_fs(offset):
        return lambda r, z, k: (r, z ^ offset, k)

    def to_rep(shift):
        return lambda r, z, k: ((r + shift) % reps, z, k)

    def to_core(r, z, k):
        return r, z, k ^ 1

    def to_y(shift):
        return lambda r, z, k: (r, z, ((k // 2 + shift) % n_y) * 2 + k % 2)

    def part_of(weight, mine, units_axis, q):
        count = weight.shape[units_axis] // 2
        first = lax.slice_in_dim(weight, 0, count, axis=units_axis)
        second = lax.slice_in_dim(weight, count, 2 * count, axis=units_axis)
        width = weight.shape[1 - units_axis] // reps
        start = ((rep - q) % reps) * width

        def cut(value):
            return lax.dynamic_slice_in_dim(value, start, width, 1 - units_axis)

        return jnp.where(lower == mine, cut(first), cut(second)).astype(low)

    def pair_part(mine, q):
        return jnp.stack([part_of(w, mine, 1, q).T for w in (gate_weight, up_weight)])

    top = down_scale.astype(low)
    rest = down_scale - top.astype(jnp.float32)
    middle = rest.astype(low)
    bottom = (rest - middle.astype(jnp.float32)).astype(low)
    terms = jnp.concatenate(
        [jnp.stack([top, middle, bottom]), jnp.zeros((SCALE_ROWS - 3, top.shape[0]), low)]
    )

    def down_piece(mine, q):
        width = terms.shape[1] // reps
        own = lax.dynamic_slice_in_dim(terms, ((rep - q) % reps) * width, width, 1)
        return jnp.concatenate([part_of(down_weight, mine, 0, q), own])

    def line(part):
        carried = {0: part(True, 0), -1: part(False, 0)}
        for s, source, offset in plan:
            carried[s] = move(carried[source], to_fs(offset))
        blocks = {0: [carried[0]] + [part(True, q) for q in range(1, reps)]}
        for s in slots[1:]:
            blocks[s] = [carried[s]] + [move(carried[s], to_rep(q)) for q in range(1, reps)]
        return blocks

    flat = tokens.astype(jnp.float32)
    mean_square = jnp.mean(flat * flat, axis=-1, keepdims=True)
    inverse = lax.rsqrt(mean_square + 1e-06)
    normed = (flat * inverse * norm_gain).astype(low)
    rows, depth = normed.shape
    own, other = [], []
    for base in (normed, move(normed, to_fs(mirror))):
        across_y = [base] + [move(base, to_y(-k)) for k in range(1, n_y)]
        across_y = jnp.concatenate(across_y)
        own.append(across_y)
        other.append(move(across_y, to_core))
    group = jnp.concatenate(own + other)

    pairs = line(pair_part)
    downs = line(down_piece)

    k_block = gate_weight.shape[0]
    k_piece = k_block // reps

    def some(chosen):
        starts = [
            (f ^ s) * k_block + ((rep - q) % reps) * k_piece for s in chosen for q in range(reps)
        ]
        return starts, [p for s in chosen for p in pairs[s]]

    scale_pair = jnp.stack([gate_scale, up_scale])
    units = scale_pair.shape[1] // 2
    scale_pair = jnp.where(lower, scale_pair[:, :units], scale_pair[:, units:])
    sums = hidden_part(group, *some(slots[:-1]), None, None)
    hidden = hidden_part(group, *some(slots[-1:]), sums, scale_pair)
    hidden_own, hidden_other = jnp.split(hidden, 2)

    def product(value, s):
        return jnp.concatenate(
            [
                jnp.dot(value, d[:units], preferred_element_type=jnp.float32).astype(low)
                for d in downs[s]
            ],
            axis=1,
        )

    kept, back = {}, {}
    for s in slots:
        total = move(product(hidden_other, s), to_core).astype(jnp.float32)
        total += product(hidden_own, s).astype(jnp.float32)
        total = total.reshape(2, n_y, rows, total.shape[-1])
        sent = total[:, 1:].astype(low)
        total = total[:, 0]
        for k in range(1, n_y):
            total += move(sent[:, k - 1], to_y(k)).astype(jnp.float32)
        kept[s] = total[0]
        back[s] = move(total[1].astype(low), to_fs(mirror))

    n_block = down_weight.shape[1]
    n_piece = n_block // reps
    mixed = jnp.zeros((rows, depth), low)
    for s in slots:
        total = kept[s] + back[s ^ mirror].astype(jnp.float32)
        for q in range(reps):
            scale = jnp.sum(downs[s][q][units : units + 3].astype(jnp.float32), axis=0)
            piece = (total[:, q * n_piece : (q + 1) * n_piece] * scale).astype(low)
            start = (f ^ s) * n_block + ((rep - q) % reps) * n_piece
            mixed = lax.dynamic_update_slice(mixed, piece, (0, start))
    return mixed


def layer(sizes, *args):
    return shards(sizes, *args)


def solution(mesh):
    in_specs = (
        P(("rep", "fs", "tp"), None),
        P(),
        P("fs", "tp"),
        P("tp"),
        P("fs", "tp"),
        P("tp"),
        P("tp", "fs"),
        P("fs"),
    )
    out_specs = P(("rep", "fs", "tp"), None)
    sizes = tuple(mesh.shape[name] for name in AXES)
    body = functools.partial(layer, sizes)
    return jax.shard_map(body, mesh=mesh, in_specs=in_specs, out_specs=out_specs, check_vma=False)
```

time: 408 us -> 235 us (0.58)
  the two profiles are of different devices: /device:TPU:0 before, /device:TPU:8 now
where the time goes in v1:
time: 235 us; the launch traced here: 233 us
  waiting for transfers between devices  108 us (46%)
  local copies, waits for them, and re-layouts  37.8 us (16%)
  starting transfers between devices  29.1 us (12%)
  other arithmetic  23.2 us (10%)
  Pallas kernels  18.5 us (8%)
  matrix products  15.5 us (7%)
    ppermute x29, waiting for transfers between devices, move(): return lax.ppermute(value, AXES, pairs)  108 us
    ppermute x29, starting transfers between devices, move(): return lax.ppermute(value, AXES, pairs)  29.1 us
    unnamed x102, local copies, waits for them, and re-layouts  21.8 us
    pallas_call x2, Pallas kernels, hidden_part(): pl.pallas_call(functools.partial(hidden_kernel, len(pieces), width, align...  18.5 us
    dot_general x16, matrix products, product(): jnp.dot(value, d[:units], preferred_element_type=jnp.float32).astype(low)  15.5 us
    another operation x7, other arithmetic, pair_part(): jnp.stack([part_of(w, mine, 1, q).T for w in (gate_weight, up_weight)])  6.45 us
    slice x4, local copies, waits for them, and re-layouts, shards(): sent = total[:, 1:].astype(low)  5.39 us
  transfers between devices with their start and end apart: 29, of which 11 were waited for; matrix products, arithmetic and copies ran while one was open for 28% of the time, Pallas kernels for 5%

profile of v1, /device:TPU:8, one launch (start us, length us, event | category | flops | bytes accessed | tf_op | source)
XLA Modules:
  0.0 233.4 jit_solution(10434724086277127069)
XLA Ops:
  0.0 1.2 fusion
  1.2 2.0 constant_dynamic-update-slice_fusion.5
  3.3 1.5 collective-permute-start
  4.8 1.6 collective-permute-start.1
  6.4 2.3 fusion.65
  8.7 1.0 constant_dynamic-slice_fusion.5
  9.7 1.9 copy.22
  11.6 1.9 copy.24
  13.6 2.3 fusion.66
  17.8 1.9 fusion.5
  20.6 1.0 pad_maximum_fusion.2
  22.5 1.0 select_convert_fusion
  23.5 1.0 pad_maximum_fusion.9
  24.5 1.5 collective-permute-start.13
  25.9 4.3 %collective-permute-start.18 = (bf16[720,256]{1,0:T(8,128)(2,1)}, bf16[720,256]{1,0:T(8,128)(2,1)}, u32[]{:S(2)}, u32[]{:S(2)}) collective-permute-start(bf16[720,256]{1,0:T(8,128)(2,1)} %get-tuple-element.30), channel_id=1, source_target_pairs={{0,4},{1,5},{2,6},{3,7},{4,0},{5,1},{6,2},{7,3},{8,12},{9,13},{10,... | collective-permute-start | bytes 1105928 | tf_op jit(solution)/shard_map/ppermute | solution.py:126
  32.1 0.9 pad_maximum_fusion.3.refs_1_
  33.8 1.0 pad_maximum_fusion.4.refs_2_
  36.1 40.1 %collective-permute-done.13 = bf16[720,256]{1,0:T(8,128)(2,1)} collective-permute-done((bf16[720,256]{1,0:T(8,128)(2,1)}, bf16[720,256]{1,0:T(8,128)(2,1)}, u32[]{:S(2)}, u32[]{:S(2)}) %collective-permute-start.13) | collective-permute-done | bytes 368672 | tf_op jit(solution)/shard_map/ppermute | solution.py:126
  76.2 1.5 collective-permute-start.19
  81.3 2.0 collective-permute-start.8
  83.3 8.0 %collective-permute-done.2 = bf16[128,2048]{1,0:T(8,128)(2,1)S(1)} collective-permute-done((bf16[128,2048]{1,0:T(8,128)(2,1)S(1)}, bf16[128,2048]{1,0:T(8,128)(2,1)S(1)}, u32[]{:S(2)}, u32[]{:S(2)}) %collective-permute-start.2) | collective-permute-done | bytes 524320 | tf_op jit(solution)/shard_map/ppermute | solution.py:126
  91.4 1.8 collective-permute-start.6
  94.0 0.9 constant_dynamic-update-slice_fusion.3
  95.0 8.3 %collective-permute-done.8.refs_3_ = bf16[2,704,256]{2,1,0:T(8,128)(2,1)S(1)} collective-permute-done((bf16[2,704,256]{2,1,0:T(8,128)(2,1)S(1)}, bf16[2,704,256]{2,1,0:T(8,128)(2,1)S(1)}, u32[]{:S(2)}, u32[]{:S(2)}) %collective-permute-start.8) | collective-permute-done | bytes 720928 | tf_op jit(solution)/shard_map/ppermute | solution.py:126
  103.3 1.5 collective-permute-start.10
  106.3 10.7 %collective-permute-done.6.refs_1_ = bf16[2,704,256]{2,1,0:T(8,128)(2,1)S(1)} collective-permute-done((bf16[2,704,256]{2,1,0:T(8,128)(2,1)}, bf16[2,704,256]{2,1,0:T(8,128)(2,1)S(1)}, u32[]{:S(2)}, u32[]{:S(2)}) %collective-permute-start.6) | collective-permute-done | bytes 720928 | tf_op jit(solution)/shard_map/ppermute | solution.py:126
  117.0 1.5 collective-permute-start.7
  118.5 1.1 constant_dynamic-update-slice_fusion.1
  119.6 1.0 constant_dynamic-update-slice_fusion.refs_0_
  120.6 1.9 collective-permute-done.10.refs_6_
  122.6 15.6 %collective-permute-done.9.refs_4_ = bf16[2,704,256]{2,1,0:T(8,128)(2,1)} collective-permute-done((bf16[2,704,256]{2,1,0:T(8,128)(2,1)S(1)}, bf16[2,704,256]{2,1,0:T(8,128)(2,1)}, u32[]{:S(2)}, u32[]{:S(2)}) %collective-permute-start.9) | collective-permute-done | bytes 720928 | tf_op jit(solution)/shard_map/ppermute | solution.py:126
  138.1 10.7 %hidden.2.refs_3_ = f32[2,1024,704]{2,1,0:T(8,128)} custom-call(s32[6]{0:T(128)} %stack.87.offsets, bf16[1024,2048]{1,0:T(8,128)(2,1)} %constant_dynamic-update-slice_fusion.refs_0_, bf16[2,704,256]{2,1,0:T(8,128)(2,1)} %pad_maximum_fusion.3.refs_1_, bf16[2,704,256]{2,1,0:T(8,128)(2,1)} %pad_maximum_fusion.4.refs_2_, bf16[2,704,256]{2,1,0:T(8,128)(2,1)} %copy-done.39, ...), custom_call_target="tpu_custom_call" | custom-call | flops 4429185024 | bytes 10092544 | tf_op jit(solution)/shard_map/hidden/pallas_call | solution.py:70
  148.8 1.4 collective-permute-done.7.refs_2_
  151.1 7.8 %hidden.3 = bf16[1024,704]{1,0:T(8,128)(2,1)} custom-call(s32[2]{0:T(128)} %pad_add_fusion.offsets, bf16[1024,2048]{1,0:T(8,128)(2,1)} %constant_dynamic-update-slice_fusion.refs_0_, bf16[2,704,256]{2,1,0:T(8,128)(2,1)} %copy-done.19, bf16[2,704,256]{2,1,0:T(8,128)(2,1)} %copy-done.20, f32[2,1024,704]{2,1,0:T(8,128)} %hidden.2.refs_3_, f32[2,704]{1,0:T(2,128)} %fusion.62.refs_4_), custom_call_target="tpu_custom_call" | custom-call | flops 1476395008 | bytes 7208960 | tf_op jit(solution)/shard_map/hidden/pallas_call | solution.py:70
  158.9 1.7 convolution_convert_fusion.13
  161.0 1.1 convolution_convert_fusion.12
  164.6 1.4 convolution_convert_fusion.7
  166.6 1.4 convolution_convert_fusion.11
  171.1 1.1 convolution_convert_fusion.4
  172.2 2.1 convolution_convert_fusion.5
  174.4 1.1 convolution_convert_fusion.8
  175.5 2.1 convolution_convert_fusion.9
  178.5 1.3 slice.230
  180.7 1.4 slice.225
  182.1 1.2 convert_add_fusion.2
  184.0 1.4 slice.218
  185.4 1.3 copy.38
  187.3 1.2 convert_add_fusion.3
  189.2 1.3 slice.213
  191.3 1.6 collective-permute-start.25
  193.6 1.4 copy.37
  194.9 2.0 copy.36
  198.1 1.3 copy.34
  199.4 1.5 collective-permute-start.12
  201.6 1.0 bitcast_add_fusion.1
  202.7 1.2 collective-permute-start.28
  203.9 8.6 %collective-permute-done.12 = bf16[2,128,512]{2,1,0:T(8,128)(2,1)S(1)} collective-permute-done((bf16[2,128,512]{2,1,0:T(8,128)(2,1)}, bf16[2,128,512]{2,1,0:T(8,128)(2,1)S(1)}, u32[]{:S(2)}, u32[]{:S(2)}) %collective-permute-start.12) | collective-permute-done | bytes 262176 | tf_op jit(solution)/shard_map/ppermute | solution.py:126
  212.6 1.2 collective-permute-start.27
  213.8 1.0 bitcast_add_fusion.2
  214.8 1.0 collective-permute-start.17
  215.8 1.0 bitcast_add_fusion
  216.9 1.2 collective-permute-start.26
  218.0 11.7 %collective-permute-done.17 = bf16[128,512]{1,0:T(8,128)(2,1)S(1)} collective-permute-done((bf16[128,512]{1,0:T(8,128)(2,1)S(1)}, bf16[128,512]{1,0:T(8,128)(2,1)S(1)}, u32[]{:S(2)}, u32[]{:S(2)}) %collective-permute-start.17) | collective-permute-done | bytes 131104 | tf_op jit(solution)/shard_map/ppermute | solution.py:126
  229.8 1.9 collective-permute-done.26
  (199 shorter events, 29.6 us)
Async XLA Ops:
  3.3 76.5 %collective-permute-start = (bf16[128,2048]{1,0:T(8,128)(2,1)S(1)}, bf16[128,2048]{1,0:T(8,128)(2,1)S(1)}, u32[]{:S(2)}, u32[]{:S(2)}) collective-permute-start(bf16[128,2048]{1,0:T(8,128)(2,1)S(1)} %get-tuple-element.8), channel_id=1, source_target_pairs={{0,2},{1,3},{2,0},{3,1},{4,6},{5,7},{6,4},{7,5},{8,10},{9,11},{10,... | collective-permute-start | bytes 1572872 | tf_op jit(solution)/shard_map/ppermute | solution.py:126
  4.8 73.7 %collective-permute-start.1 = (bf16[128,2048]{1,0:T(8,128)(2,1)S(1)}, bf16[128,2048]{1,0:T(8,128)(2,1)S(1)}, u32[]{:S(2)}, u32[]{:S(2)}) collective-permute-start(bf16[128,2048]{1,0:T(8,128)(2,1)S(1)} %get-tuple-element.8), channel_id=1, source_target_pairs={{0,12},{1,13},{2,14},{3,15},{4,8},{5,9},{6,10},{7,11},{8,4},{9,5},... | collective-permute-start | bytes 1572872 | tf_op jit(solution)/shard_map/ppermute | solution.py:126
  16.9 2.9 %copy-start.10 = (bf16[256,704]{0,1:T(8,128)(2,1)S(1)}, bf16[256,704]{0,1:T(8,128)(2,1)}, u32[]{:S(2)}) copy-start(bf16[256,704]{0,1:T(8,128)(2,1)} %copy.26) | copy-start | bytes 1081348
  17.8 1.9 copy-start.11
  19.8 2.2 copy-start.17
  21.5 59.7 %collective-permute-start.5 = (bf16[2,704,256]{2,1,0:T(8,128)(2,1)}, bf16[2,704,256]{2,1,0:T(8,128)(2,1)}, u32[]{:S(2)}, u32[]{:S(2)}) collective-permute-start(bf16[2,704,256]{2,1,0:T(8,128)(2,1)} %pad_maximum_fusion.2), channel_id=1, source_target_pairs={{0,12},{1,13},{2,14},{3,15},{4,8},{5,9},{6,10},{7,11},{8,4},{9,5},... | collective-permute-start | bytes 2162696 | tf_op jit(solution)/shard_map/ppermute | solution.py:126
  22.5 7.7 %copy-start.8 = (bf16[256,704]{1,0:T(8,128)(2,1)S(1)}, bf16[256,704]{1,0:T(8,128)(2,1)}, u32[]{:S(2)}) copy-start(bf16[256,704]{1,0:T(8,128)(2,1)} %get-tuple-element.38) | copy-start | bytes 1081348
  23.5 6.7 %copy-start.12 = (bf16[704,256]{1,0:T(8,128)(2,1)}, bf16[704,256]{1,0:T(8,128)(2,1)S(1)}, u32[]{:S(2)}) copy-start(bf16[704,256]{1,0:T(8,128)(2,1)S(1)} %get-tuple-element.17) | copy-start | bytes 1081348
  24.5 51.7 %collective-permute-start.13 = (bf16[720,256]{1,0:T(8,128)(2,1)}, bf16[720,256]{1,0:T(8,128)(2,1)}, u32[]{:S(2)}, u32[]{:S(2)}) collective-permute-start(bf16[720,256]{1,0:T(8,128)(2,1)} %get-tuple-element.31), channel_id=1, source_target_pairs={{0,12},{1,13},{2,14},{3,15},{4,8},{5,9},{6,10},{7,11},{8,4},{9,5},... | collective-permute-start | bytes 1105928 | tf_op jit(solution)/shard_map/ppermute | solution.py:126
  25.9 50.3 %collective-permute-start.18 = (bf16[720,256]{1,0:T(8,128)(2,1)}, bf16[720,256]{1,0:T(8,128)(2,1)}, u32[]{:S(2)}, u32[]{:S(2)}) collective-permute-start(bf16[720,256]{1,0:T(8,128)(2,1)} %get-tuple-element.30), channel_id=1, source_target_pairs={{0,4},{1,5},{2,6},{3,7},{4,0},{5,1},{6,2},{7,3},{8,12},{9,13},{10,... | collective-permute-start | bytes 1105928 | tf_op jit(solution)/shard_map/ppermute | solution.py:126
  30.9 2.2 copy-start.28
  30.9 2.1 copy-start.29
  31.8 2.0 copy-start.16
  76.2 15.1 %collective-permute-start.22 = (bf16[720,256]{1,0:T(8,128)(2,1)}, bf16[720,256]{1,0:T(8,128)(2,1)S(1)}, u32[]{:S(2)}, u32[]{:S(2)}) collective-permute-start(bf16[720,256]{1,0:T(8,128)(2,1)} %collective-permute-done.13), channel_id=1, source_target_pairs={{0,4},{1,5},{2,6},{3,7},{4,0},{5,1},{6,2},{7,3},{8,12},{9,13},{10,... | collective-permute-start | bytes 1105928 | tf_op jit(solution)/shard_map/ppermute | solution.py:126
  76.2 16.9 %collective-permute-start.19 = (bf16[720,256]{1,0:T(8,128)(2,1)}, bf16[720,256]{1,0:T(8,128)(2,1)S(1)}, u32[]{:S(2)}, u32[]{:S(2)}) collective-permute-start(bf16[720,256]{1,0:T(8,128)(2,1)} %collective-permute-done.18), channel_id=1, source_target_pairs={{0,16},{1,17},{2,18},{3,19},{4,20},{5,21},{6,22},{7,23},{8,24},{9,... | collective-permute-start | bytes 1105928 | tf_op jit(solution)/shard_map/ppermute | solution.py:126
  78.5 12.8 %collective-permute-start.2 = (bf16[128,2048]{1,0:T(8,128)(2,1)S(1)}, bf16[128,2048]{1,0:T(8,128)(2,1)S(1)}, u32[]{:S(2)}, u32[]{:S(2)}) collective-permute-start(bf16[128,2048]{1,0:T(8,128)(2,1)S(1)} %collective-permute-done.1), channel_id=1, source_target_pairs={{0,2},{1,3},{2,0},{3,1},{4,6},{5,7},{6,4},{7,5},{8,10},{9,11},{10,... | collective-permute-start | bytes 1572872 | tf_op jit(solution)/shard_map/ppermute | solution.py:126
  79.7 1.5 copy-start.18
  79.7 14.3 %collective-permute-start.14 = (bf16[720,256]{1,0:T(8,128)(2,1)}, bf16[720,256]{1,0:T(8,128)(2,1)S(1)}, u32[]{:S(2)}, u32[]{:S(2)}) collective-permute-start(bf16[720,256]{1,0:T(8,128)(2,1)} %collective-permute-done.13), channel_id=1, source_target_pairs={{0,16},{1,17},{2,18},{3,19},{4,20},{5,21},{6,22},{7,23},{8,24},{9,... | collective-permute-start | bytes 1105928 | tf_op jit(solution)/shard_map/ppermute | solution.py:126
  81.3 22.1 %collective-permute-start.8 = (bf16[2,704,256]{2,1,0:T(8,128)(2,1)S(1)}, bf16[2,704,256]{2,1,0:T(8,128)(2,1)S(1)}, u32[]{:S(2)}, u32[]{:S(2)}) collective-permute-start(bf16[2,704,256]{2,1,0:T(8,128)(2,1)S(1)} %copy-done.18), channel_id=1, source_target_pairs={{0,4},{1,5},{2,6},{3,7},{4,0},{5,1},{6,2},{7,3},{8,12},{9,13},{10,... | collective-permute-start | bytes 2162696 | tf_op jit(solution)/shard_map/ppermute | solution.py:126
  91.2 27.3 %collective-permute-start.3 = (bf16[256,2048]{1,0:T(8,128)(2,1)S(1)}, bf16[256,2048]{1,0:T(8,128)(2,1)S(1)}, u32[]{:S(2)}, u32[]{:S(2)}) collective-permute-start(bf16[256,2048]{1,0:T(8,128)(2,1)S(1)} %pad_maximum_fusion), channel_id=1, source_target_pairs={{0,1},{1,0},{2,3},{3,2},{4,5},{5,4},{6,7},{7,6},{8,9},{9,8},{10,11... | collective-permute-start | bytes 3145736 | tf_op jit(solution)/shard_map/ppermute | solution.py:126
  91.3 15.0 %copy-start.31 = (bf16[720,256]{1,0:T(8,128)(2,1)}, bf16[720,256]{1,0:T(8,128)(2,1)S(1)}, u32[]{:S(2)}) copy-start(bf16[720,256]{1,0:T(8,128)(2,1)S(1)} %collective-permute-done.22) | copy-start | bytes 1105924
  91.4 25.6 %collective-permute-start.6 = (bf16[2,704,256]{2,1,0:T(8,128)(2,1)}, bf16[2,704,256]{2,1,0:T(8,128)(2,1)S(1)}, u32[]{:S(2)}, u32[]{:S(2)}) collective-permute-start(bf16[2,704,256]{2,1,0:T(8,128)(2,1)} %collective-permute-done.5.refs_5_), channel_id=1, source_target_pairs={{0,4},{1,5},{2,6},{3,7},{4,0},{5,1},{6,2},{7,3},{8,12},{9,13},{10,... | collective-permute-start | bytes 2162696 | tf_op jit(solution)/shard_map/ppermute | solution.py:126
  93.2 26.4 %copy-start.33 = (bf16[720,256]{1,0:T(8,128)(2,1)}, bf16[720,256]{1,0:T(8,128)(2,1)S(1)}, u32[]{:S(2)}) copy-start(bf16[720,256]{1,0:T(8,128)(2,1)S(1)} %collective-permute-done.19) | copy-start | bytes 1105924
  93.2 11.7 %collective-permute-start.23 = (bf16[720,256]{1,0:T(8,128)(2,1)S(1)}, bf16[720,256]{1,0:T(8,128)(2,1)S(1)}, u32[]{:S(2)}, u32[]{:S(2)}) collective-permute-start(bf16[720,256]{1,0:T(8,128)(2,1)S(1)} %collective-permute-done.22), channel_id=1, source_target_pairs={{0,16},{1,17},{2,18},{3,19},{4,20},{5,21},{6,22},{7,23},{8,24},{9,... | collective-permute-start | bytes 1105928 | tf_op jit(solution)/shard_map/ppermute | solution.py:126
  94.0 25.6 %copy-start.35 = (bf16[720,256]{1,0:T(8,128)(2,1)}, bf16[720,256]{1,0:T(8,128)(2,1)S(1)}, u32[]{:S(2)}) copy-start(bf16[720,256]{1,0:T(8,128)(2,1)S(1)} %collective-permute-done.14) | copy-start | bytes 1105924
  94.0 25.6 %collective-permute-start.4 = (bf16[256,2048]{1,0:T(8,128)(2,1)S(1)}, bf16[256,2048]{1,0:T(8,128)(2,1)S(1)}, u32[]{:S(2)}, u32[]{:S(2)}) collective-permute-start(bf16[256,2048]{1,0:T(8,128)(2,1)S(1)} %pad_maximum_fusion.1), channel_id=1, source_target_pairs={{0,1},{1,0},{2,3},{3,2},{4,5},{5,4},{6,7},{7,6},{8,9},{9,8},{10,11... | collective-permute-start | bytes 3145736 | tf_op jit(solution)/shard_map/ppermute | solution.py:126
  103.3 16.2 %copy-start.39 = (bf16[2,704,256]{2,1,0:T(8,128)(2,1)}, bf16[2,704,256]{2,1,0:T(8,128)(2,1)S(1)}, u32[]{:S(2)}) copy-start(bf16[2,704,256]{2,1,0:T(8,128)(2,1)S(1)} %collective-permute-done.8.refs_3_) | copy-start | bytes 2162692
  103.3 19.2 %collective-permute-start.10 = (bf16[2,704,256]{2,1,0:T(8,128)(2,1)}, bf16[2,704,256]{2,1,0:T(8,128)(2,1)S(1)}, u32[]{:S(2)}, u32[]{:S(2)}) collective-permute-start(bf16[2,704,256]{2,1,0:T(8,128)(2,1)} %collective-permute-done.5.refs_5_), channel_id=1, source_target_pairs={{0,16},{1,17},{2,18},{3,19},{4,20},{5,21},{6,22},{7,23},{8,24},{9,... | collective-permute-start | bytes 2162696 | tf_op jit(solution)/shard_map/ppermute | solution.py:126
  104.8 57.7 %copy-start.37 = (bf16[720,256]{1,0:T(8,128)(2,1)}, bf16[720,256]{1,0:T(8,128)(2,1)S(1)}, u32[]{:S(2)}) copy-start(bf16[720,256]{1,0:T(8,128)(2,1)S(1)} %collective-permute-done.23) | copy-start | bytes 1105924
  104.8 33.3 %collective-permute-start.9 = (bf16[2,704,256]{2,1,0:T(8,128)(2,1)S(1)}, bf16[2,704,256]{2,1,0:T(8,128)(2,1)}, u32[]{:S(2)}, u32[]{:S(2)}) collective-permute-start(bf16[2,704,256]{2,1,0:T(8,128)(2,1)S(1)} %collective-permute-done.8.refs_3_), channel_id=1, source_target_pairs={{0,16},{1,17},{2,18},{3,19},{4,20},{5,21},{6,22},{7,23},{8,24},{9,... | collective-permute-start | bytes 2162696 | tf_op jit(solution)/shard_map/ppermute | solution.py:126
  117.0 3.6 %copy-start.19 = (bf16[2,704,256]{2,1,0:T(8,128)(2,1)}, bf16[2,704,256]{2,1,0:T(8,128)(2,1)S(1)}, u32[]{:S(2)}) copy-start(bf16[2,704,256]{2,1,0:T(8,128)(2,1)S(1)} %collective-permute-done.6.refs_1_) | copy-start | bytes 2162692
  117.0 33.2 %collective-permute-start.7 = (bf16[2,704,256]{2,1,0:T(8,128)(2,1)S(1)}, bf16[2,704,256]{2,1,0:T(8,128)(2,1)S(1)}, u32[]{:S(2)}, u32[]{:S(2)}) collective-permute-start(bf16[2,704,256]{2,1,0:T(8,128)(2,1)S(1)} %collective-permute-done.6.refs_1_), channel_id=1, source_target_pairs={{0,16},{1,17},{2,18},{3,19},{4,20},{5,21},{6,22},{7,23},{8,24},{9,... | collective-permute-start | bytes 2162696 | tf_op jit(solution)/shard_map/ppermute | solution.py:126
  122.6 15.6 %copy-start.40 = (bf16[2,704,256]{2,1,0:T(8,128)(2,1)}, bf16[2,704,256]{2,1,0:T(8,128)(2,1)S(1)}, u32[]{:S(2)}) copy-start(bf16[2,704,256]{2,1,0:T(8,128)(2,1)S(1)} %collective-permute-done.10.refs_6_) | copy-start | bytes 2162692
  148.8 10.0 %copy-start.13 = (bf16[704,256]{1,0:T(8,128)(2,1)S(1)}, bf16[704,256]{1,0:T(8,128)(2,1)}, u32[]{:S(2)}) copy-start(bf16[704,256]{1,0:T(8,128)(2,1)} %copy-done.12) | copy-start | bytes 1081348
  158.9 1.7 copy-start.9
  158.9 2.1 copy-start.22
  163.6 14.0 %collective-permute-start.24 = (bf16[512,512]{0,1:T(8,128)(2,1)S(1)}, bf16[512,512]{0,1:T(8,128)(2,1)S(1)}, u32[]{:S(2)}, u32[]{:S(2)}) collective-permute-start(bf16[512,512]{0,1:T(8,128)(2,1)S(1)} %pad_maximum_fusion.8), channel_id=1, source_target_pairs={{0,1},{1,0},{2,3},{3,2},{4,5},{5,4},{6,7},{7,6},{8,9},{9,8},{10,11... | collective-permute-start | bytes 1572872 | tf_op jit(solution)/shard_map/ppermute | solution.py:126
  164.5 1.6 copy-start.36
  166.1 13.8 %collective-permute-start.20 = (bf16[512,512]{0,1:T(8,128)(2,1)S(1)}, bf16[512,512]{0,1:T(8,128)(2,1)S(1)}, u32[]{:S(2)}, u32[]{:S(2)}) collective-permute-start(bf16[512,512]{0,1:T(8,128)(2,1)S(1)} %pad_maximum_fusion.7), channel_id=1, source_target_pairs={{0,1},{1,0},{2,3},{3,2},{4,5},{5,4},{6,7},{7,6},{8,9},{9,8},{10,11... | collective-permute-start | bytes 1572872 | tf_op jit(solution)/shard_map/ppermute | solution.py:126
  166.6 3.7 %copy-start.38 = (bf16[720,256]{1,0:T(8,128)(2,1)S(1)}, bf16[720,256]{1,0:T(8,128)(2,1)}, u32[]{:S(2)}) copy-start(bf16[720,256]{1,0:T(8,128)(2,1)} %copy-done.37) | copy-start | bytes 1105924
  168.9 13.2 %collective-permute-start.15 = (bf16[512,512]{0,1:T(8,128)(2,1)}, bf16[512,512]{0,1:T(8,128)(2,1)}, u32[]{:S(2)}, u32[]{:S(2)}) collective-permute-start(bf16[512,512]{0,1:T(8,128)(2,1)} %pad_maximum_fusion.6), channel_id=1, source_target_pairs={{0,1},{1,0},{2,3},{3,2},{4,5},{5,4},{6,7},{7,6},{8,9},{9,8},{10,11... | collective-permute-start | bytes 1572872 | tf_op jit(solution)/shard_map/ppermute | solution.py:126
  170.2 17.1 %collective-permute-start.11 = (bf16[512,512]{0,1:T(8,128)(2,1)}, bf16[512,512]{0,1:T(8,128)(2,1)}, u32[]{:S(2)}, u32[]{:S(2)}) collective-permute-start(bf16[512,512]{0,1:T(8,128)(2,1)} %pad_maximum_fusion.5), channel_id=1, source_target_pairs={{0,1},{1,0},{2,3},{3,2},{4,5},{5,4},{6,7},{7,6},{8,9},{9,8},{10,11... | collective-permute-start | bytes 1572872 | tf_op jit(solution)/shard_map/ppermute | solution.py:126
  178.4 1.6 copy-start
  178.5 1.4 copy-start.27
  180.7 2.6 %copy-start.1 = (f32[2,2,128,512]{2,1,0,3:T(2,128)}, f32[2,2,128,512]{2,1,0,3:T(2,128)S(1)}, u32[]{:S(2)}) copy-start(f32[2,2,128,512]{2,1,0,3:T(2,128)S(1)} %reshape.35) | copy-start | bytes 3145732
  184.0 4.5 %copy-start.2 = (f32[2,2,128,512]{2,1,0,3:T(2,128)}, f32[2,2,128,512]{2,1,0,3:T(2,128)S(1)}, u32[]{:S(2)}) copy-start(f32[2,2,128,512]{2,1,0,3:T(2,128)S(1)} %reshape.34) | copy-start | bytes 3145732
  184.0 1.4 copy-start.7
  184.0 3.2 %copy-start.23 = (bf16[512,256]{0,1:T(8,128)(2,1)S(1)}, bf16[512,256]{0,1:T(8,128)(2,1)}, u32[]{:S(2)}) copy-start(bf16[512,256]{0,1:T(8,128)(2,1)} %convolution_convert_fusion.12) | copy-start | bytes 786436
  186.8 14.9 %collective-permute-start.21 = (bf16[2,128,512]{2,1,0:T(8,128)(2,1)}, bf16[2,128,512]{2,1,0:T(8,128)(2,1)}, u32[]{:S(2)}, u32[]{:S(2)}) collective-permute-start(bf16[2,128,512]{2,1,0:T(8,128)(2,1)} %bitcast.81), channel_id=1, source_target_pairs={{0,2},{1,3},{2,0},{3,1},{4,6},{5,7},{6,4},{7,5},{8,10},{9,11},{10,... | collective-permute-start | bytes 786440 | tf_op jit(solution)/shard_map/ppermute | solution.py:126
  189.2 4.4 %copy-start.3 = (f32[2,2,128,512]{2,1,0,3:T(2,128)}, f32[2,2,128,512]{2,1,0,3:T(2,128)S(1)}, u32[]{:S(2)}) copy-start(f32[2,2,128,512]{2,1,0,3:T(2,128)S(1)} %reshape.33) | copy-start | bytes 3145732
  189.2 1.4 copy-start.4
  189.2 3.7 %slice-start = ((f32[2,2,128,512]{2,1,0,3:T(2,128)}), f32[2,1,128,512]{2,1,0,3:T(1,128)S(1)}, s32[]{:S(2)}) async-start(f32[2,2,128,512]{2,1,0,3:T(2,128)} %copy-done), calls=%async_computation | async-start | bytes 1048576 | tf_op jit(solution)/shard_map/slice | solution.py:224
  190.5 3.0 %slice-start.1 = ((f32[2,2,128,512]{2,1,0,3:T(2,128)}), f32[2,1,128,512]{2,1,0,3:T(1,128)S(1)}, s32[]{:S(2)}) async-start(f32[2,2,128,512]{2,1,0,3:T(2,128)} %copy-done.1), calls=%async_computation.1 | async-start | bytes 1048576 | tf_op jit(solution)/shard_map/slice | solution.py:224
  191.3 6.2 %slice-start.2 = ((f32[2,2,128,512]{2,1,0,3:T(2,128)}), f32[2,1,128,512]{2,1,0,3:T(1,128)S(1)}, s32[]{:S(2)}) async-start(f32[2,2,128,512]{2,1,0,3:T(2,128)} %copy-done.2), calls=%async_computation.2 | async-start | bytes 1048576 | tf_op jit(solution)/shard_map/slice | solution.py:224
  191.3 24.5 %collective-permute-start.25 = (bf16[2,128,512]{2,1,0:T(8,128)(2,1)S(1)}, bf16[2,128,512]{2,1,0:T(8,128)(2,1)}, u32[]{:S(2)}, u32[]{:S(2)}) collective-permute-start(bf16[2,128,512]{2,1,0:T(8,128)(2,1)S(1)} %bitcast.88), channel_id=1, source_target_pairs={{0,2},{1,3},{2,0},{3,1},{4,6},{5,7},{6,4},{7,5},{8,10},{9,11},{10,... | collective-permute-start | bytes 786440 | tf_op jit(solution)/shard_map/ppermute | solution.py:126
  194.9 3.2 %copy-start.6 = (bf16[2,1,128,512]{2,1,0,3:T(2,128)(2,1)S(1)}, bf16[2,1,128,512]{2,1,0,3:T(2,128)(2,1)}, u32[]{:S(2)}) copy-start(bf16[2,1,128,512]{2,1,0,3:T(2,128)(2,1)} %slice.213) | copy-start | bytes 786436
  194.9 6.0 %slice-start.3 = ((f32[2,2,128,512]{2,1,0,3:T(2,128)}), f32[2,1,128,512]{2,1,0,3:T(1,128)S(1)}, s32[]{:S(2)}) async-start(f32[2,2,128,512]{2,1,0,3:T(2,128)} %copy-done.3), calls=%async_computation.3 | async-start | bytes 1048576 | tf_op jit(solution)/shard_map/slice | solution.py:224
  196.9 4.7 %copy-start.5 = (f32[2,1,128,512]{3,2,0,1:T(8,128)S(1)}, f32[2,1,128,512]{3,2,0,1:T(8,128)}, u32[]{:S(2)}) copy-start(f32[2,1,128,512]{3,2,0,1:T(8,128)} %copy.37) | copy-start | bytes 1572868
  196.9 16.8 %collective-permute-start.16 = (bf16[2,128,512]{2,1,0:T(8,128)(2,1)}, bf16[2,128,512]{2,1,0:T(8,128)(2,1)}, u32[]{:S(2)}, u32[]{:S(2)}) collective-permute-start(bf16[2,128,512]{2,1,0:T(8,128)(2,1)} %bitcast.82), channel_id=1, source_target_pairs={{0,2},{1,3},{2,0},{3,1},{4,6},{5,7},{6,4},{7,5},{8,10},{9,11},{10,... | collective-permute-start | bytes 786440 | tf_op jit(solution)/shard_map/ppermute | solution.py:126
  199.4 13.1 %collective-permute-start.12 = (bf16[2,128,512]{2,1,0:T(8,128)(2,1)}, bf16[2,128,512]{2,1,0:T(8,128)(2,1)S(1)}, u32[]{:S(2)}, u32[]{:S(2)}) collective-permute-start(bf16[2,128,512]{2,1,0:T(8,128)(2,1)} %bitcast.83), channel_id=1, source_target_pairs={{0,2},{1,3},{2,0},{3,1},{4,6},{5,7},{6,4},{7,5},{8,10},{9,11},{10,... | collective-permute-start | bytes 786440 | tf_op jit(solution)/shard_map/ppermute | solution.py:126
  202.7 29.2 %collective-permute-start.28 = (bf16[128,512]{1,0:T(8,128)(2,1)S(1)}, bf16[128,512]{1,0:T(8,128)(2,1)S(1)}, u32[]{:S(2)}, u32[]{:S(2)}) collective-permute-start(bf16[128,512]{1,0:T(8,128)(2,1)S(1)} %fusion.44), channel_id=1, source_target_pairs={{0,12},{1,13},{2,14},{3,15},{4,8},{5,9},{6,10},{7,11},{8,4},{9,5},... | collective-permute-start | bytes 393224 | tf_op jit(solution)/shard_map/ppermute | solution.py:126
  212.6 19.2 %collective-permute-start.27 = (bf16[128,512]{1,0:T(8,128)(2,1)S(1)}, bf16[128,512]{1,0:T(8,128)(2,1)S(1)}, u32[]{:S(2)}, u32[]{:S(2)}) collective-permute-start(bf16[128,512]{1,0:T(8,128)(2,1)S(1)} %fusion.43), channel_id=1, source_target_pairs={{0,12},{1,13},{2,14},{3,15},{4,8},{5,9},{6,10},{7,11},{8,4},{9,5},... | collective-permute-start | bytes 393224 | tf_op jit(solution)/shard_map/ppermute | solution.py:126
  214.8 14.9 %collective-permute-start.17 = (bf16[128,512]{1,0:T(8,128)(2,1)S(1)}, bf16[128,512]{1,0:T(8,128)(2,1)S(1)}, u32[]{:S(2)}, u32[]{:S(2)}) collective-permute-start(bf16[128,512]{1,0:T(8,128)(2,1)S(1)} %fusion.41), channel_id=1, source_target_pairs={{0,12},{1,13},{2,14},{3,15},{4,8},{5,9},{6,10},{7,11},{8,4},{9,5},... | collective-permute-start | bytes 393224 | tf_op jit(solution)/shard_map/ppermute | solution.py:126
  216.9 14.8 %collective-permute-start.26 = (bf16[128,512]{1,0:T(8,128)(2,1)S(1)}, bf16[128,512]{1,0:T(8,128)(2,1)S(1)}, u32[]{:S(2)}, u32[]{:S(2)}) collective-permute-start(bf16[128,512]{1,0:T(8,128)(2,1)S(1)} %fusion.42), channel_id=1, source_target_pairs={{0,12},{1,13},{2,14},{3,15},{4,8},{5,9},{6,10},{7,11},{8,4},{9,5},... | collective-permute-start | bytes 393224 | tf_op jit(solution)/shard_map/ppermute | solution.py:126
  (10 other events, 10.8 us)
